TPU v7x, 32 devices: a whole 2x2x4 slice. The times are simulated.
32 devices in a mesh: grp: 2 (over y), sp: 4 (over z), dp: 4 (over x, core).
Axes of the slice: x: 2, y: 2, z: 4, core: 2. Of those that a mesh axis runs over, the one named last changes fastest.
Arguments:
- gate_input: bfloat16 [8, 1536, 2048], P(('grp', 'dp'), 'sp'), parts along dimension 0, may hold values from -6 to 6
- value_input: bfloat16 [8, 1536, 2048], P(('grp', 'dp'), 'sp'), parts along dimension 0, may hold values from -6 to 6
- norm_gain: bfloat16 [2048], replicated, may hold values from 0.099609375 to 1.8984375
- norm_bias: bfloat16 [2048], replicated, may hold values from -2.5 to 2.5
- mix_weight: bfloat16 [16, 1024, 1024], P('sp', 'dp'), may hold values from -0.1875 to 0.1875
- mix_bias: bfloat16 [16, 1024], P('sp'), may hold values from 0.099609375 to 1.8984375
Outputs:
- gated: bfloat16 [8, 1536, 2048], P(('grp', 'dp'), 'sp'), parts along dimension 0
There are 2 independent parts, one for each index of `grp`. A program takes and returns all parts, laid end to end along the dimension named above; an argument that names none is the same for every part. Nothing has to cross between parts.
All inputs are finite; a program needn't handle non-finite values.
Results may differ from a plain program's by a relative error of at most 0.0053.
Values may be sent and summed in bfloat16 or wider, within the bound.
A program may use at most 64 MiB of HBM per device.

v0:
```python
import jax
import jax.numpy as jnp
from jax import lax
from jax.sharding import PartitionSpec as P

GD = 128
BLK = 1024


def mix_groups(normed_ex, mix_weight, mix_bias):
    seqs, length, local_width = normed_ex.shape
    groups_here = mix_weight.shape[0]
    nblocks = -(-length // BLK)
    padded = jnp.pad(normed_ex, ((0, 0), (0, nblocks * BLK - length), (0, 0)))
    blocks = padded.reshape(seqs * nblocks, BLK, groups_here, GD)
    piece = lax.all_gather(mix_weight, "dp", axis=1, tiled=True)
    count = piece.shape[1]
    rows = lax.iota(jnp.int32, count)
    cols = lax.iota(jnp.int32, BLK)
    keep = cols[None, :] <= rows[:, None]
    masked = jnp.where(keep[None], piece, jnp.zeros_like(piece))
    term = jnp.einsum("gts,bsgc->btgc", masked, blocks, preferred_element_type=jnp.float32)
    bias_rows = mix_bias.astype(jnp.float32)
    mixed = term + bias_rows.T[None, :, :, None]
    mixed = mixed.reshape(seqs, nblocks * BLK, local_width)[:, :length]
    return mixed.astype(jnp.bfloat16)


def body(gate_input, value_input, norm_gain, norm_bias, mix_weight, mix_bias):
    act = jax.nn.gelu(value_input.astype(jnp.float32))
    mean = jnp.mean(act, axis=-1, keepdims=True)
    var = jnp.mean(jnp.square(act - mean), axis=-1, keepdims=True)
    normed = (
        (act - mean) * lax.rsqrt(var + 1e-06) * norm_gain.astype(jnp.float32)
        + norm_bias.astype(jnp.float32)
    ).astype(jnp.bfloat16)
    normed_ex = lax.all_to_all(normed, "sp", split_axis=2, concat_axis=1, tiled=True)
    mixed = mix_groups(normed_ex, mix_weight, mix_bias)
    returned = lax.all_to_all(mixed, "sp", split_axis=1, concat_axis=2, tiled=True)
    gated = jax.nn.gelu(gate_input.astype(jnp.float32)) * returned.astype(jnp.float32)
    return gated.astype(jnp.bfloat16)


def solution(mesh):
    placed = (
        P(("grp", "dp"), "sp", None),
        P(("grp", "dp"), "sp", None),
        P(),
        P(),
        P("sp", "dp", None),
        P("sp", None),
    )
    return jax.shard_map(
        body, mesh=mesh, in_specs=placed, out_specs=P(("grp", "dp"), "sp", None), check_vma=False
    )
```

profile of v0, /device:TPU:0, one launch (start us, length us, event | category | flops | bytes accessed | tf_op | source)
XLA Modules:
  0.0 239.9 jit_solution(9603832664579578522)
XLA Ops:
  11.3 1.5 add_convert_fusion
  12.9 30.1 %copy.35 = bf16[1,384,2048]{1,0,2:T(2,128)(2,1)S(1)} copy(bf16[1,384,2048]{1,2,0:T(8,128)(2,1)S(1)} %add_convert_fusion) | data formatting | bytes 3145728 | tf_op jit(solution)/shard_map/convert_element_type | solution.py:36
  43.5 34.4 %reduce.2 = bf16[2048,384]{1,0:T(8,128)(2,1)} reduce(bf16[2048,1,384]{2,1,0:T(2,128)(2,1)S(1)} %bitcast.31, bf16[]{:T(256)} %broadcast.85), dimensions={1}, to_apply=%bitcast.30.reduce_sub_computation | reduce | bytes 3145730
  77.9 3.7 %reshape.69 = bf16[4,2,98304]{2,1,0:T(2,128)(2,1)} reshape(bf16[2048,384]{1,0:T(8,128)(2,1)} %reduce.2) | data formatting | bytes 3145728
  81.7 6.3 %all-to-all-start = ((bf16[4,2,98304]{2,1,0:T(2,128)(2,1)}), bf16[4,2,98304]{2,1,0:T(2,128)(2,1)}, u32[]{:S(2)}, u32[]{:S(2)}) async-start(bf16[4,2,98304]{2,1,0:T(2,128)(2,1)} %reshape.69), calls=%async_computation | async-start | bytes 3145728 | tf_op jit(solution)/shard_map/all_to_all | solution.py:37
  89.3 35.8 %all-to-all-done = bf16[4,2,98304]{2,1,0:T(2,128)(2,1)} async-done(((bf16[4,2,98304]{2,1,0:T(2,128)(2,1)}), bf16[4,2,98304]{2,1,0:T(2,128)(2,1)}, u32[]{:S(2)}, u32[]{:S(2)}) %all-to-all-start) | async-done | bytes 1572896 | tf_op jit(solution)/shard_map/all_to_all | solution.py:37
  125.1 3.1 %reshape.70 = bf16[2048,1,384]{2,1,0:T(2,128)(2,1)S(1)} reshape(bf16[4,2,98304]{2,1,0:T(2,128)(2,1)} %all-to-all-done) | data formatting | bytes 3145728
  129.6 2.6 %copy.19 = bf16[1,4,384,512]{3,2,1,0:T(8,128)(2,1)} copy(bf16[1,4,384,512]{2,3,1,0:T(8,128)(2,1)} %bitcast.36) | data formatting | bytes 3145728 | tf_op jit(solution)/shard_map/all_to_all | solution.py:37
  132.2 1.6 pad.4
  133.8 2.1 reshape.64
  135.9 8.1 %fusion.4 = bf16[2,1024,4,128]{1,3,0,2:T(8,128)(2,1)} fusion(f32[1024,4]{0,1:T(4,128)S(1)} %convert_bitcast_fusion.1, bf16[4,1024,1024]{2,1,0:T(8,128)(2,1)} %all-gather.2.cloned.1.call-done, pred[1024,1024]{1,0:T(8,128)(4,1)S(1)} %copy-done.2, bf16[2,1024,4,128]{3,2,1,0:T(4,128)(2,1)} %reshape.64), kind=kOutput, calls=%fused_computation.13 | convolution fusion | flops 2153775104 | bytes 13647872 | tf_op jit(solution)/shard_map/gts,bsgc->btgc/dot_general | solution.py:22
  144.0 3.1 %copy.21 = bf16[2,1024,4,128]{3,2,1,0:T(4,128)(2,1)S(1)} copy(bf16[2,1024,4,128]{1,3,0,2:T(8,128)(2,1)} %fusion.4) | data formatting | bytes 4194304 | tf_op jit(solution)/shard_map/convert.5
  147.2 2.2 reshape.65
  150.8 11.7 %copy.34 = bf16[1,1536,512]{2,0,1:T(2,128)(2,1)S(1)} copy(bf16[1,1536,512]{2,1,0:T(8,128)(2,1)S(1)} %slice-done) | data formatting | bytes 3145728 | tf_op jit(solution)/shard_map/slice | solution.py:25
  162.5 11.1 %reduce.3 = bf16[1536,512]{1,0:T(8,128)(2,1)} reduce(bf16[1536,1,512]{2,1,0:T(2,128)(2,1)S(1)} %bitcast.32, bf16[]{:T(256)} %broadcast.85), dimensions={1}, to_apply=%bitcast.29.reduce_sub_computation | reduce | bytes 3145730
  173.5 4.3 %reshape.71 = bf16[4,2,98304]{2,1,0:T(2,128)(2,1)} reshape(bf16[1536,512]{1,0:T(8,128)(2,1)} %reduce.3) | data formatting | bytes 3145728
  177.8 4.3 %all-to-all-start.1 = ((bf16[4,2,98304]{2,1,0:T(2,128)(2,1)}), bf16[4,2,98304]{2,1,0:T(2,128)(2,1)}, u32[]{:S(2)}, u32[]{:S(2)}) async-start(bf16[4,2,98304]{2,1,0:T(2,128)(2,1)} %reshape.71), calls=%async_computation.1 | async-start | bytes 3145728 | tf_op jit(solution)/shard_map/all_to_all | solution.py:39
  182.2 1.6 copy.16
  183.7 35.0 %all-to-all-done.1 = bf16[4,2,98304]{2,1,0:T(2,128)(2,1)} async-done(((bf16[4,2,98304]{2,1,0:T(2,128)(2,1)}), bf16[4,2,98304]{2,1,0:T(2,128)(2,1)}, u32[]{:S(2)}, u32[]{:S(2)}) %all-to-all-start.1) | async-done | bytes 1572896 | tf_op jit(solution)/shard_map/all_to_all | solution.py:39
  218.7 3.1 %reshape.72 = bf16[1536,1,512]{2,1,0:T(2,128)(2,1)S(1)} reshape(bf16[4,2,98304]{2,1,0:T(2,128)(2,1)} %all-to-all-done.1) | data formatting | bytes 3145728
  222.2 2.1 convert_bitcast_fusion
  224.3 2.4 copy.24
  226.7 3.8 %fusion.12 = bf16[1,384,2048]{1,2,0:T(8,128)(2,1)} fusion(bf16[1,384,2048]{1,2,0:T(8,128)(2,1)} %copy.16, f32[1,384,4,512]{1,3,2,0:T(8,128)S(1)} %copy.24), kind=kLoop, calls=%fused_computation.22 | loop fusion | flops 8650752 | bytes 6291456 | tf_op jit(solution)/shard_map/convert_element_type | solution.py:41
  230.5 2.6 %copy.25 = bf16[1,384,2048]{2,1,0:T(8,128)(2,1)} copy(bf16[1,384,2048]{1,2,0:T(8,128)(2,1)} %fusion.12) | data formatting | bytes 3145728 | tf_op jit(solution)/shard_map/convert_element_type | solution.py:41
  (29 shorter events, 9.9 us)
Async XLA Ops:
  6.5 1.4 copy-start
  6.5 2.3 copy-start.4
  6.5 2.3 copy-start.5
  6.5 129.4 %all-gather.2.cloned.1.call-start = ((), (), s32[]{:S(2)}) async-start(), calls=%async_computation.2 | async-start | bytes 10485760 | tf_op jit(solution)/shard_map/all_gather | solution.py:16
  77.9 11.4 %copy-start.3 = (bf16[4,1024]{1,0:T(4,128)(2,1)S(1)}, bf16[4,1024]{1,0:T(4,128)(2,1)}, u32[]{:S(2)}) copy-start(bf16[4,1024]{1,0:T(4,128)(2,1)} %param.11) | copy-start | bytes 24580
  81.7 43.4 %all-to-all-start = ((bf16[4,2,98304]{2,1,0:T(2,128)(2,1)}), bf16[4,2,98304]{2,1,0:T(2,128)(2,1)}, u32[]{:S(2)}, u32[]{:S(2)}) async-start(bf16[4,2,98304]{2,1,0:T(2,128)(2,1)} %reshape.69), calls=%async_computation | async-start | bytes 3145728 | tf_op jit(solution)/shard_map/all_to_all | solution.py:37
  132.2 3.7 %copy-start.2 = (pred[1024,1024]{1,0:T(8,128)(4,1)S(1)}, pred[1024,1024]{1,0:T(8,128)(4,1)}, u32[]{:S(2)}) copy-start(pred[1024,1024]{1,0:T(8,128)(4,1)} %iota_compare_fusion) | copy-start | bytes 3145732
  149.4 1.4 slice-start
  173.5 8.6 %copy-start.1 = (bf16[1,384,2048]{2,1,0:T(8,128)(2,1)S(1)}, bf16[1,384,2048]{2,1,0:T(8,128)(2,1)}, u32[]{:S(2)}) copy-start(bf16[1,384,2048]{2,1,0:T(8,128)(2,1)} %param.6) | copy-start | bytes 4718596
  177.8 40.9 %all-to-all-start.1 = ((bf16[4,2,98304]{2,1,0:T(2,128)(2,1)}), bf16[4,2,98304]{2,1,0:T(2,128)(2,1)}, u32[]{:S(2)}, u32[]{:S(2)}) async-start(bf16[4,2,98304]{2,1,0:T(2,128)(2,1)} %reshape.71), calls=%async_computation.1 | async-start | bytes 3145728 | tf_op jit(solution)/shard_map/all_to_all | solution.py:39
Sparse Core Ops, SparseCore 0:
  8.9 60.9 all-gather.1
where the time goes:
time: 241 us; the launch traced here: 240 us
  local copies, waits for them, and re-layouts  79.4 us (33%)
  waiting for transfers between devices  71.5 us (30%)
  other arithmetic  56.7 us (24%)
  between operations  13.5 us (6%)
  starting transfers between devices  10.7 us (4%)
  matrix products  8.09 us (3%)
    unnamed x2, other arithmetic  45.5 us
    all_to_all x1, waiting for transfers between devices, body(): lax.all_to_all(normed, 'sp', split_axis=2, concat_axis=1, tiled=True)  35.8 us
    all_to_all x1, waiting for transfers between devices, body(): lax.all_to_all(mixed, 'sp', split_axis=1, concat_axis=2, tiled=True)  35 us
    convert_element_type x1, local copies, waits for them, and re-layouts, body(): normed = ((act - mean) * lax.rsqrt(var + 1e-06) * norm_gain.astype(jnp.fl...  30.1 us
    unnamed x20, local copies, waits for them, and re-layouts  19.2 us
    slice x3, local copies, waits for them, and re-layouts, mix_groups(): mixed = mixed.reshape(seqs, nblocks * BLK, local_width)[:, :length]  13.1 us
    dot_general x1, matrix products, mix_groups(): jnp.einsum('gts,bsgc->btgc', masked, blocks, preferred_element_type=jnp.f...  8.09 us
    all_to_all x1, starting transfers between devices, body(): lax.all_to_all(normed, 'sp', split_axis=2, concat_axis=1, tiled=True)  6.35 us
  transfers between devices with their start and end apart: 3, of which 2 were waited for; matrix products, arithmetic and copies ran while one was open for 36% of the time, Pallas kernels for 0%

commit v1 on v0

--- a/solution.py
+++ b/solution.py
@@ -2,6 +2,7 @@
 import jax.numpy as jnp
 from jax import lax
 from jax.sharding import PartitionSpec as P
+from jax.lax import all_to_all, axis_size
 
 GD = 128
 BLK = 1024
@@ -36,7 +37,13 @@
     ).astype(jnp.bfloat16)
     normed_ex = lax.all_to_all(normed, "sp", split_axis=2, concat_axis=1, tiled=True)
     mixed = mix_groups(normed_ex, mix_weight, mix_bias)
-    returned = lax.all_to_all(mixed, "sp", split_axis=1, concat_axis=2, tiled=True)
+    extend_patches_all = lambda local_block, ax_name: jnp.concatenate(
+        all_to_all(
+            jnp.stack(jnp.split(local_block, axis_size(ax_name), axis=1), axis=0), ax_name, 0, 0
+        ),
+        axis=2,
+    )
+    returned = extend_patches_all(mixed, "sp")
     gated = jax.nn.gelu(gate_input.astype(jnp.float32)) * returned.astype(jnp.float32)
     return gated.astype(jnp.bfloat16)
 

time: 241 us -> 211 us (0.88)
  local copies, waits for them, and re-layouts: 79.4 us -> 60.1 us
  other arithmetic: 56.7 us -> 47 us
    slice x3 -> x0, local copies, waits for them, and re-layouts: 13.1 us -> none  [mix_groups(): mixed = mixed.reshape(seqs, nblocks * BLK, local_width)[:, :length]]
    unnamed x2 -> x1, other arithmetic: 45.5 us -> 34.4 us
    unnamed x20 -> x18, local copies, waits for them, and re-layouts: 19.2 us -> 11.9 us
  transfers between devices with their start and end apart: 3 -> 3, of which waited for: 2 -> 2; matrix products, arithmetic and copies ran while one was open for 36% -> 42% of each run, Pallas kernels for 0% -> 0%
where the time goes in v1:
time: 211 us; the launch traced here: 210 us
  waiting for transfers between devices  71.4 us (34%)
  local copies, waits for them, and re-layouts  60.1 us (28%)
  other arithmetic  47 us (22%)
  between operations  13.5 us (6%)
  starting transfers between devices  9.91 us (5%)
  matrix products  8.1 us (4%)
    all_to_all x1, waiting for transfers between devices, body(): lax.all_to_all(normed, 'sp', split_axis=2, concat_axis=1, tiled=True)  35.8 us
    all_to_all x1, waiting for transfers between devices, body(): all_to_all(jnp.stack(jnp.split(local_block, axis_size(ax_name), axis=1),...  34.9 us
    unnamed x1, other arithmetic  34.4 us
    convert_element_type x1, local copies, waits for them, and re-layouts, body(): normed = ((act - mean) * lax.rsqrt(var + 1e-06) * norm_gain.astype(jnp.fl...  30.1 us
    unnamed x18, local copies, waits for them, and re-layouts  11.9 us
    dot_general x1, matrix products, mix_groups(): jnp.einsum('gts,bsgc->btgc', masked, blocks, preferred_element_type=jnp.f...  8.1 us
    all_to_all x1, starting transfers between devices, body(): lax.all_to_all(normed, 'sp', split_axis=2, concat_axis=1, tiled=True)  6.35 us
  transfers between devices with their start and end apart: 3, of which 2 were waited for; matrix products, arithmetic and copies ran while one was open for 42% of the time, Pallas kernels for 0%

profile of v1, /device:TPU:0, one launch (start us, length us, event | category | flops | bytes accessed | tf_op | source)
XLA Modules:
  0.0 209.9 jit_solution(4532512922358735839)
XLA Ops:
  10.0 1.3 multiply_reduce_fusion
  11.3 1.5 add_convert_fusion
  12.9 30.1 %copy.34 = bf16[1,384,2048]{1,0,2:T(2,128)(2,1)S(1)} copy(bf16[1,384,2048]{1,2,0:T(8,128)(2,1)S(1)} %add_convert_fusion) | data formatting | bytes 3145728 | tf_op jit(solution)/shard_map/convert_element_type | solution.py:37
  43.6 34.4 %reduce.2 = bf16[2048,384]{1,0:T(8,128)(2,1)} reduce(bf16[2048,1,384]{2,1,0:T(2,128)(2,1)S(1)} %bitcast.33, bf16[]{:T(256)} %broadcast.85), dimensions={1}, to_apply=%bitcast.32.reduce_sub_computation | reduce | bytes 3145730
  78.0 3.7 %reshape.68 = bf16[4,2,98304]{2,1,0:T(2,128)(2,1)} reshape(bf16[2048,384]{1,0:T(8,128)(2,1)} %reduce.2) | data formatting | bytes 3145728
  81.7 6.3 %all-to-all-start = ((bf16[4,2,98304]{2,1,0:T(2,128)(2,1)}), bf16[4,2,98304]{2,1,0:T(2,128)(2,1)}, u32[]{:S(2)}, u32[]{:S(2)}) async-start(bf16[4,2,98304]{2,1,0:T(2,128)(2,1)} %reshape.68), calls=%async_computation | async-start | bytes 3145728 | tf_op jit(solution)/shard_map/all_to_all | solution.py:38
  89.4 35.8 %all-to-all-done = bf16[4,2,98304]{2,1,0:T(2,128)(2,1)} async-done(((bf16[4,2,98304]{2,1,0:T(2,128)(2,1)}), bf16[4,2,98304]{2,1,0:T(2,128)(2,1)}, u32[]{:S(2)}, u32[]{:S(2)}) %all-to-all-start) | async-done | bytes 1572896 | tf_op jit(solution)/shard_map/all_to_all | solution.py:38
  125.1 3.1 %reshape.69 = bf16[2048,1,384]{2,1,0:T(2,128)(2,1)S(1)} reshape(bf16[4,2,98304]{2,1,0:T(2,128)(2,1)} %all-to-all-done) | data formatting | bytes 3145728
  128.2 1.4 copy.28
  129.6 2.6 %copy.22 = bf16[1,4,384,512]{3,2,1,0:T(8,128)(2,1)} copy(bf16[1,4,384,512]{2,3,1,0:T(8,128)(2,1)} %bitcast.36) | data formatting | bytes 3145728 | tf_op jit(solution)/shard_map/all_to_all | solution.py:38
  132.2 1.6 pad.4
  133.8 2.1 reshape.64
  135.9 8.1 %fusion.4 = bf16[2,1024,4,128]{1,3,0,2:T(8,128)(2,1)} fusion(f32[1024,4]{0,1:T(4,128)S(1)} %convert_bitcast_fusion.1, bf16[4,1024,1024]{2,1,0:T(8,128)(2,1)} %all-gather.2.cloned.1.call-done, pred[1024,1024]{1,0:T(8,128)(4,1)S(1)} %copy-done.2, bf16[2,1024,4,128]{3,2,1,0:T(4,128)(2,1)} %reshape.64), kind=kOutput, calls=%fused_computation.13 | convolution fusion | flops 2153775104 | bytes 13647872 | tf_op jit(solution)/shard_map/gts,bsgc->btgc/dot_general | solution.py:23
  144.0 3.1 %copy.24 = bf16[2,1024,4,128]{3,2,1,0:T(4,128)(2,1)S(1)} copy(bf16[2,1024,4,128]{1,3,0,2:T(8,128)(2,1)} %fusion.4) | data formatting | bytes 4194304 | tf_op jit(solution)/shard_map/convert.4
  147.2 2.2 %reshape.65 = bf16[1,2048,512]{2,1,0:T(8,128)(2,1)} reshape(bf16[2,1024,4,128]{3,2,1,0:T(4,128)(2,1)S(1)} %copy.24) | data formatting | bytes 4194304 | tf_op jit(solution)/shard_map/reshape | solution.py:26
  149.4 1.5 slice_bitcast_fusion.3
  150.9 1.4 pad_maximum_fusion
  152.2 3.6 %all-to-all-start.1 = ((bf16[4,1,384,512]{3,2,1,0:T(8,128)(2,1)}), bf16[4,1,384,512]{3,2,1,0:T(8,128)(2,1)S(1)}, u32[]{:S(2)}, u32[]{:S(2)}) async-start(bf16[4,1,384,512]{3,2,1,0:T(8,128)(2,1)} %pad_maximum_fusion), calls=%async_computation.1 | async-start | bytes 3145728 | tf_op jit(solution)/shard_map/all_to_all | solution.py:41
  155.8 1.6 copy.19
  157.4 34.9 %all-to-all-done.1 = bf16[4,1,384,512]{3,2,1,0:T(8,128)(2,1)S(1)} async-done(((bf16[4,1,384,512]{3,2,1,0:T(8,128)(2,1)}), bf16[4,1,384,512]{3,2,1,0:T(8,128)(2,1)S(1)}, u32[]{:S(2)}, u32[]{:S(2)}) %all-to-all-start.1) | async-done | bytes 1572896 | tf_op jit(solution)/shard_map/all_to_all | solution.py:41
  192.3 2.1 convert_bitcast_fusion
  194.4 2.4 %copy.25 = f32[1,384,4,512]{1,3,2,0:T(8,128)S(1)} copy(f32[1,384,4,512]{3,1,0,2:T(8,128)} %convert_bitcast_fusion) | data formatting | bytes 6291456 | tf_op jit(solution)/shard_map/convert_element_type | solution.py:47
  196.7 3.8 %fusion.12 = bf16[1,384,2048]{1,2,0:T(8,128)(2,1)} fusion(bf16[1,384,2048]{1,2,0:T(8,128)(2,1)} %copy.19, f32[1,384,4,512]{1,3,2,0:T(8,128)S(1)} %copy.25), kind=kLoop, calls=%fused_computation.22 | loop fusion | flops 8650752 | bytes 6291456 | tf_op jit(solution)/shard_map/convert_element_type | solution.py:48
  200.5 2.6 %copy.26 = bf16[1,384,2048]{2,1,0:T(8,128)(2,1)} copy(bf16[1,384,2048]{1,2,0:T(8,128)(2,1)} %fusion.12) | data formatting | bytes 3145728 | tf_op jit(solution)/shard_map/convert_element_type | solution.py:48
  (24 shorter events, 5.3 us)
Async XLA Ops:
  6.5 1.4 copy-start
  6.5 2.3 %copy-start.4 = (bf16[2048]{0:T(1024)(128)(2,1)S(1)}, bf16[2048]{0:T(1024)(128)(2,1)}, u32[]{:S(2)}) copy-start(bf16[2048]{0:T(1024)(128)(2,1)} %param.8) | copy-start | bytes 12292
  6.5 2.3 %copy-start.5 = (bf16[2048]{0:T(1024)(128)(2,1)S(1)}, bf16[2048]{0:T(1024)(128)(2,1)}, u32[]{:S(2)}) copy-start(bf16[2048]{0:T(1024)(128)(2,1)} %param.9) | copy-start | bytes 12292
  6.5 129.4 %all-gather.2.cloned.1.call-start = ((), (), s32[]{:S(2)}) async-start(), calls=%async_computation.2 | async-start | bytes 10485760 | tf_op jit(solution)/shard_map/all_gather | solution.py:17
  78.0 11.4 %copy-start.3 = (bf16[4,1024]{1,0:T(4,128)(2,1)S(1)}, bf16[4,1024]{1,0:T(4,128)(2,1)}, u32[]{:S(2)}) copy-start(bf16[4,1024]{1,0:T(4,128)(2,1)} %param.11) | copy-start | bytes 24580
  81.7 43.4 %all-to-all-start = ((bf16[4,2,98304]{2,1,0:T(2,128)(2,1)}), bf16[4,2,98304]{2,1,0:T(2,128)(2,1)}, u32[]{:S(2)}, u32[]{:S(2)}) async-start(bf16[4,2,98304]{2,1,0:T(2,128)(2,1)} %reshape.68), calls=%async_computation | async-start | bytes 3145728 | tf_op jit(solution)/shard_map/all_to_all | solution.py:38
  132.2 3.7 %copy-start.2 = (pred[1024,1024]{1,0:T(8,128)(4,1)S(1)}, pred[1024,1024]{1,0:T(8,128)(4,1)}, u32[]{:S(2)}) copy-start(pred[1024,1024]{1,0:T(8,128)(4,1)} %iota_compare_fusion) | copy-start | bytes 3145732
  150.8 4.9 %copy-start.1 = (bf16[1,384,2048]{2,1,0:T(8,128)(2,1)S(1)}, bf16[1,384,2048]{2,1,0:T(8,128)(2,1)}, u32[]{:S(2)}) copy-start(bf16[1,384,2048]{2,1,0:T(8,128)(2,1)} %param.6) | copy-start | bytes 4718596
  152.2 40.1 %all-to-all-start.1 = ((bf16[4,1,384,512]{3,2,1,0:T(8,128)(2,1)}), bf16[4,1,384,512]{3,2,1,0:T(8,128)(2,1)S(1)}, u32[]{:S(2)}, u32[]{:S(2)}) async-start(bf16[4,1,384,512]{3,2,1,0:T(8,128)(2,1)} %pad_maximum_fusion), calls=%async_computation.1 | async-start | bytes 3145728 | tf_op jit(solution)/shard_map/all_to_all | solution.py:41
Sparse Core Ops, SparseCore 0:
  8.9 60.9 all-gather.1
